TPU v7x, 32 devices: a whole 2x2x4 slice. The times are simulated.
32 devices in a mesh: sp: 4 (over y, x), tp: 8 (over z, core).
Axes of the slice: x: 2, y: 2, z: 4, core: 2. Of those that a mesh axis runs over, the one named last changes fastest.
Arguments:
- latent: bfloat16 [2048, 4096], P(('sp', 'tp')), may hold values from -6 to 6
- context: bfloat16 [512, 4096], P('sp'), may hold values from -6 to 6
- condition: float32 [4096], replicated, may hold values from -6 to 6
- context_condition: float32 [4096], replicated, may hold values from -6 to 6
- modulation: bfloat16 [3, 4096, 4096], P(None, 'sp', 'tp'), may hold values from -0.09375 to 0.09375
- query_weight: bfloat16 [4096, 4096], P(None, 'tp'), as said below
- key_weight: bfloat16 [4096, 4096], P(None, 'tp'), as said below
- value_weight: bfloat16 [4096, 4096], P(None, 'tp'), may hold values from -0.09375 to 0.09375
- lambdas: float32 [16], P('tp'), may hold values from 0.3 to 0.8
- context_lift: float32 [16], P('tp'), may hold values from 1.5 to 3
- head_gain: float32 [256], replicated, may hold values from 0.1 to 1.9
- output_weight: bfloat16 [4096, 4096], P('tp'), may hold values from -0.09375 to 0.09375
Outputs:
- result: bfloat16 [2048, 4096], P(('sp', 'tp'))
Inputs may be any that keep to these rules, and one draw needn't show every extreme that they name: `query_weight`: entries lie within 200 / sqrt(4096) in magnitude. `key_weight`: entries lie within 6 / sqrt(4096) in magnitude.
All inputs are finite; a program needn't handle non-finite values.
Results may differ from a plain program's by a relative error of at most 0.025.
Values may be sent and summed in bfloat16 or wider, within the bound.
A program may use at most 64 MiB of HBM per device.

v0:
```python
import math
import jax
import jax.numpy as jnp
from jax import lax
from jax.sharding import PartitionSpec as P

GRID_W = 64
ROPE_BASE = 10000.0
EPSILON = 1e-05


def modulate(tokens_in, offset, scaling):
    values = tokens_in.astype(jnp.float32)
    center = jnp.mean(values, axis=-1, keepdims=True)
    spread = jnp.mean(jnp.square(values - center), axis=-1, keepdims=True)
    normed = (values - center) * lax.rsqrt(spread + EPSILON)
    return (normed * (1.0 + scaling) + offset).astype(jnp.bfloat16)


def rotate(tensor, places):
    number, head_count, head_width = tensor.shape
    quarter = head_width // 4
    eighth = head_width // 8
    inverse = ROPE_BASE ** (-jnp.arange(eighth, dtype=jnp.float32) / eighth)
    grid_row = (places // GRID_W).astype(jnp.float32)
    grid_col = (places % GRID_W).astype(jnp.float32)
    angles = jnp.stack([grid_row[:, None] * inverse, grid_col[:, None] * inverse], axis=1)
    cosine = jnp.cos(angles)[:, None, None, :, :]
    sine_table = jnp.sin(angles)[:, None, None, :, :]
    pieces = tensor.reshape(number, head_count, 2, 2, quarter)
    first_half = pieces[..., :eighth]
    second = pieces[..., eighth:]
    turned = jnp.concatenate(
        [first_half * cosine - second * sine_table, second * cosine + first_half * sine_table],
        axis=-1,
    )
    return turned.reshape(number, head_count, head_width)


def absorb(state_in, key_block, queries, lift_term, scale_factor):
    running_max, running_sum, running_out = state_in
    key_count = key_block.shape[0]
    head_count = queries.shape[1]
    head_width = 2 * queries.shape[3]
    local_width = head_count * head_width
    key_part = key_block[:, :local_width].reshape(key_count, head_count, 2, head_width // 2)
    value_part = key_block[:, local_width:].reshape(key_count, head_count, head_width)
    scores = (
        jnp.einsum("qhmd,khmd->mqhk", queries, key_part, preferred_element_type=jnp.float32)
        * scale_factor
        + lift_term
    )
    new_max = jnp.maximum(running_max, jnp.max(scores, axis=-1))
    fading = jnp.exp(running_max - new_max)
    weights = jnp.exp(scores - new_max[..., None])
    new_sum = running_sum * fading + jnp.sum(weights, axis=-1)
    new_out = running_out * fading[..., None] + jnp.einsum(
        "mqhk,khd->mqhd",
        weights.astype(jnp.bfloat16),
        value_part,
        preferred_element_type=jnp.float32,
    )
    return (new_max, new_sum, new_out)


def shards(
    latent,
    context,
    condition,
    context_condition,
    modulation,
    query_weight,
    key_weight,
    value_weight,
    lambdas,
    context_lift,
    head_gain,
    output_weight,
):
    sp_index = lax.axis_index("sp")
    rows_block = modulation.shape[1]
    silu_pair = jax.nn.silu(jnp.stack([condition, context_condition])).astype(jnp.bfloat16)
    own_rows = lax.dynamic_slice_in_dim(silu_pair, sp_index * rows_block, rows_block, 1)
    partial_mod = jnp.einsum(
        "cd,rde->cre", own_rows, modulation, preferred_element_type=jnp.float32
    )
    summed = lax.psum(partial_mod, "sp")
    mod_vectors = lax.all_gather(summed, "tp", axis=2, tiled=True)
    head_count = lambdas.shape[0]
    head_width = query_weight.shape[1] // head_count
    half_width = head_width // 2
    local_width = head_count * head_width
    scale_factor = half_width ** (-0.5)
    normed = modulate(latent, mod_vectors[0, 0], mod_vectors[0, 1])
    projection = jnp.concatenate([query_weight, key_weight, value_weight], axis=1)
    projected = jnp.dot(
        lax.all_gather(normed, "tp", axis=0, tiled=True),
        projection,
        preferred_element_type=jnp.float32,
    ).astype(jnp.bfloat16)
    block_tokens = projected.shape[0]
    places = sp_index * block_tokens + jnp.arange(block_tokens, dtype=jnp.int32)
    queries = rotate(
        projected[:, :local_width]
        .astype(jnp.float32)
        .reshape(block_tokens, head_count, head_width),
        places,
    )
    queries = queries.astype(jnp.bfloat16).reshape(block_tokens, head_count, 2, half_width)
    latent_keys = rotate(
        projected[:, local_width : 2 * local_width]
        .astype(jnp.float32)
        .reshape(block_tokens, head_count, head_width),
        places,
    )
    latent_keys = latent_keys.astype(jnp.bfloat16).reshape(block_tokens, local_width)
    packed = jnp.concatenate([latent_keys, projected[:, 2 * local_width :]], axis=1)
    normed_context = modulate(context, mod_vectors[1, 0], mod_vectors[1, 1])
    own_context = jnp.dot(
        normed_context, projection[:, local_width:], preferred_element_type=jnp.float32
    ).astype(jnp.bfloat16)
    context_packed = lax.all_gather(own_context, "sp", axis=0, tiled=True)
    initial = (
        jnp.full((2, block_tokens, head_count), -jnp.inf, jnp.float32),
        jnp.zeros((2, block_tokens, head_count), jnp.float32),
        jnp.zeros((2, block_tokens, head_count, head_width), jnp.float32),
    )
    state_now = absorb(initial, context_packed, queries, context_lift[:, None], scale_factor)
    segment = lax.all_gather(packed, "sp", axis=0, tiled=True)
    length = segment.shape[0]
    block_len = math.gcd(length, 1024)
    stacked = segment.reshape(length // block_len, block_len, segment.shape[1])

    def one_block(state_step, block_rows):
        return (absorb(state_step, block_rows, queries, 0.0, scale_factor), None)

    running_max, running_sum, running_out = lax.scan(one_block, state_now, stacked)[0]
    means = running_out / running_sum[..., None]
    difference = means[0] - lambdas[None, :, None] * means[1]
    scaled = (
        difference
        * lax.rsqrt(jnp.mean(jnp.square(difference), axis=-1, keepdims=True) + EPSILON)
        * head_gain
    )
    attended = scaled.astype(jnp.bfloat16).reshape(block_tokens, local_width)
    mixture = lax.psum_scatter(
        jnp.dot(attended, output_weight, preferred_element_type=jnp.float32).astype(jnp.bfloat16),
        "tp",
        scatter_dimension=0,
        tiled=True,
    ).astype(jnp.float32)
    return (latent.astype(jnp.float32) + mod_vectors[0, 2] * mixture).astype(jnp.bfloat16)


def solution(mesh):
    in_specs = (
        P(("sp", "tp"), None),
        P("sp", None),
        P(),
        P(),
        P(None, "sp", "tp"),
        P(None, "tp"),
        P(None, "tp"),
        P(None, "tp"),
        P("tp"),
        P("tp"),
        P(),
        P("tp", None),
    )
    out_specs = P(("sp", "tp"), None)
    return jax.shard_map(shards, mesh=mesh, in_specs=in_specs, out_specs=out_specs, check_vma=False)
```

profile of v0, /device:TPU:0, one launch (start us, length us, event | category | flops | bytes accessed | tf_op | source)
XLA Modules:
  0.0 269.9 jit_solution(10086001366930255042)
XLA Ops:
  6.5 1.9 copy-done
  8.4 1.3 fusion.61
  9.7 17.6 %psum.7 = f32[2,3,512]{2,0,1:T(2,128)S(1)} all-reduce(f32[2,3,512]{2,0,1:T(2,128)S(1)} %fusion.61), channel_id=1, replica_groups=mesh['sp'=4,'tp'=8] {'sp'}, use_global_device_ids=true, to_apply=%region_0.1 | all-reduce | flops 3072 | bytes 24576 | tf_op jit(solution)/shard_map/psum | solution.py:87
  27.3 14.1 %all_gather.12 = f32[2,3,4096]{2,0,1:T(2,128)S(1)} all-gather(f32[2,3,512]{2,0,1:T(2,128)S(1)} %psum.7), channel_id=1, replica_groups=mesh['sp'=4,'tp'=8] {'tp'}, dimensions={2}, use_global_device_ids=true | all-gather | bytes 110592 | tf_op jit(solution)/shard_map/all_gather | solution.py:88
  42.7 1.3 fusion.40
  44.1 2.1 fusion.43
  46.3 1.5 convert_reduce_fusion
  48.2 5.0 %fusion.37 = bf16[128,1024]{1,0:T(8,128)(2,1)} fusion(bf16[4096,512]{1,0:T(8,128)(2,1)} %param.21, bf16[4096,512]{1,0:T(8,128)(2,1)} %param.20, bf16[128,4096]{1,0:T(8,128)(2,1)S(1)} %copy-done.3, f32[4096]{0:T(1024)S(1)} %bitcast.120, f32[4096]{0:T(1024)S(1)} %bitcast.121, f32[128]{0:T(128)S(1)} %add_rsqrt_fusion.2, f32[128]{0:T(128)S(1)} %broadcast_multiply_fusion.3), kind=kOutput, calls=%fused_computation.47 | convolution fusion | flops 1093795840 | bytes 9733120 | tf_op jit(solution)/shard_map/dot_general | solution.py:119
  54.5 37.9 %all-gather.6.cloned.1.call-done = bf16[512,4096]{1,0:T(8,128)(2,1)} async-done(((bf16[64,4096]{1,0:T(8,128)(2,1)}), bf16[512,4096]{1,0:T(8,128)(2,1)}) %all-gather.6.cloned.1.call-update) | async-done | bytes 4194320 | tf_op jit(solution)/shard_map/all_gather | solution.py:97
  92.4 12.5 %fusion.22 = bf16[512,1536]{1,0:T(8,128)(2,1)S(1)} fusion(bf16[512,4096]{1,0:T(8,128)(2,1)} %all-gather.6.cloned.1.call-done, bf16[4096,512]{1,0:T(8,128)(2,1)} %param.21, bf16[4096,512]{1,0:T(8,128)(2,1)} %param.20, bf16[4096,512]{1,0:T(8,128)(2,1)} %param.19), kind=kOutput, calls=%fused_computation.30 | convolution fusion | flops 6480986112 | bytes 18350080 | tf_op jit(solution)/shard_map/dot_general | solution.py:96
  106.7 2.0 subtract_convert_fusion
  110.5 9.1 %all-gather.4.cloned.1.call-done = bf16[512,1024]{1,0:T(8,128)(2,1)} async-done(((bf16[128,1024]{1,0:T(8,128)(2,1)}), bf16[512,1024]{1,0:T(8,128)(2,1)}) %all-gather.4.cloned.1.call-update) | async-done | bytes 1048592 | tf_op jit(solution)/shard_map/all_gather | solution.py:122
  119.6 1.3 fusion.77
  122.3 1.8 bitcast_reduce_fusion.1
  125.1 2.0 bitcast_add_fusion.1
  127.1 46.9 %all-gather.8.cloned.1.call-done = bf16[2048,1024]{1,0:T(8,128)(2,1)} async-done(((bf16[512,1024]{1,0:T(8,128)(2,1)}), bf16[2048,1024]{1,0:T(8,128)(2,1)}) %all-gather.8.cloned.1.call-update) | async-done | bytes 4194320 | tf_op jit(solution)/shard_map/all_gather | solution.py:129
  174.0 28.7 %while.14 = (s32[]{:T(128)}, f32[2,512,2]{1,2,0:T(2,128)S(1)}, f32[2,512,2]{1,2,0:T(2,128)S(1)}, f32[2,512,2,256]{1,3,0,2:T(8,128)}, bf16[2,1024,1024]{2,1,0:T(8...) while((s32[]{:T(128)}, f32[2,512,2]{1,2,0:T(2,128)S(1)}, f32[2,512,2]{1,2,0:T(2,128)S(1)}, ...), condition=%wide.region_10.11_spmd, body=%wide.region_7.10_spmd.sunk | while | flops 1624248320 | bytes 44703824 | solution.py:137
  174.0 3.1 %constant_dynamic-slice_fusion.2 = bf16[1,1024,1024]{2,1,0:T(8,128)(2,1)} fusion(bf16[2,1024,1024]{2,1,0:T(8,128)(2,1)} %get-tuple-element.173, s32[]{:T(128)} %get-tuple-element.162), kind=kLoop, calls=%fused_computation.12.clone.1 | loop fusion | bytes 4194308 | tf_op jit(solution)/shard_map/while/body/jit(dynamic_index_in_dim)/dynamic_slice | solution.py:137
  177.1 2.9 %copy.75 = bf16[1,1024,1024]{1,2,0:T(8,128)(2,1)S(1)} copy(bf16[1,1024,1024]{2,1,0:T(8,128)(2,1)} %constant_dynamic-slice_fusion.2) | data formatting | bytes 4194304 | tf_op jit(solution)/shard_map/while/body/jit(dynamic_index_in_dim)/dynamic_slice | solution.py:137
  180.2 2.4 bitcast_reduce_fusion.3
  182.6 1.6 fusion.96
  184.2 4.2 %bitcast_add_fusion.3 = f32[2,512,2,256]{1,3,0,2:T(8,128)} fusion(f32[2,512,2,256]{1,3,0,2:T(8,128)} %get-tuple-element.165, bf16[1024,2,256,1]{0,2,3,1:T(8,128)(2,1)S(1)} %bitcast.107, bf16[2,512,2,1024]{1,3,2,0:T(8,128)(2,1)S(1)} %get-tuple-element.153, f32[2,512,2]{1,0,2:T(2,128)S(1)} %copy.76), kind=kOutput, calls=%fused_computation.7.clone.1 | convolution fusion | flops 1074790400 | bytes 9445376 | tf_op jit(solution)/shard_map/while/body/eval_jaxpr/mqhk,khd->mqhd/dot_general | solution.py:57
  188.4 3.1 %constant_dynamic-slice_fusion.2 = bf16[1,1024,1024]{2,1,0:T(8,128)(2,1)} fusion(bf16[2,1024,1024]{2,1,0:T(8,128)(2,1)} %get-tuple-element.173, s32[]{:T(128)} %get-tuple-element.162), kind=kLoop, calls=%fused_computation.12.clone.1 | loop fusion | bytes 4194308 | tf_op jit(solution)/shard_map/while/body/jit(dynamic_index_in_dim)/dynamic_slice | solution.py:137
  191.5 2.9 %copy.75 = bf16[1,1024,1024]{1,2,0:T(8,128)(2,1)S(1)} copy(bf16[1,1024,1024]{2,1,0:T(8,128)(2,1)} %constant_dynamic-slice_fusion.2) | data formatting | bytes 4194304 | tf_op jit(solution)/shard_map/while/body/jit(dynamic_index_in_dim)/dynamic_slice | solution.py:137
  194.5 2.4 bitcast_reduce_fusion.3
  196.9 1.6 fusion.96
  198.6 4.2 %bitcast_add_fusion.3 = f32[2,512,2,256]{1,3,0,2:T(8,128)} fusion(f32[2,512,2,256]{1,3,0,2:T(8,128)} %get-tuple-element.165, bf16[1024,2,256,1]{0,2,3,1:T(8,128)(2,1)S(1)} %bitcast.107, bf16[2,512,2,1024]{1,3,2,0:T(8,128)(2,1)S(1)} %get-tuple-element.153, f32[2,512,2]{1,0,2:T(2,128)S(1)} %copy.76), kind=kOutput, calls=%fused_computation.7.clone.1 | convolution fusion | flops 1074790400 | bytes 9445376 | tf_op jit(solution)/shard_map/while/body/eval_jaxpr/mqhk,khd->mqhd/dot_general | solution.py:57
  202.8 1.9 broadcast_divide_fusion
  205.5 1.3 copy-done.2
  206.8 4.3 %convolution_convert_fusion = bf16[512,4096]{1,0:T(8,128)(2,1)} fusion(bf16[512,512]{0,1:T(8,128)(2,1)S(1)} %fusion.50, bf16[512,4096]{1,0:T(8,128)(2,1)S(1)} %copy-done.2), kind=kOutput, calls=%fused_computation.23 | convolution fusion | flops 2149580800 | bytes 8912896 | tf_op jit(solution)/shard_map/dot_general | solution.py:147
  211.2 50.1 %reduce-scatter.2.cloned.1.call-done = bf16[64,4096]{1,0:T(8,128)(2,1)} async-done(((bf16[512,4096]{1,0:T(8,128)(2,1)}), bf16[64,4096]{1,0:T(8,128)(2,1)}) %reduce-scatter.2.cloned.1.call-update) | async-done | bytes 524304 | tf_op jit(solution)/shard_map/reduce_scatter | solution.py:146
  261.3 2.1 fusion.44
  (67 shorter events, 10.3 us)
Async XLA Ops:
  6.5 1.9 copy-start
  6.5 85.9 %all-gather.6.cloned.1.call-start = ((), (), s32[]{:S(2)}) async-start(), calls=%async_computation.2 | async-start | bytes 4718592 | tf_op jit(solution)/shard_map/all_gather | solution.py:97
  9.7 38.0 %copy-start.3 = (bf16[128,4096]{1,0:T(8,128)(2,1)S(1)}, bf16[128,4096]{1,0:T(8,128)(2,1)}, u32[]{:S(2)}) copy-start(bf16[128,4096]{1,0:T(8,128)(2,1)} %param.15) | copy-start | bytes 3145732
  46.2 73.4 %all-gather.4.cloned.1.call-start = ((), (), s32[]{:S(2)}) async-start(), calls=%async_computation.1 | async-start | bytes 1310720 | tf_op jit(solution)/shard_map/all_gather | solution.py:122
  53.2 120.9 %all-gather.8.cloned.1.call-start = ((), (), s32[]{:S(2)}) async-start(), calls=%async_computation.3 | async-start | bytes 5242880 | tf_op jit(solution)/shard_map/all_gather | solution.py:129
  106.7 2.3 copy-start.4
  108.7 1.7 copy-start.7
  108.7 1.8 copy-start.8
  108.8 12.4 %copy-start.5 = (bf16[512,2,2,2,32]{0,4,3,2,1:T(8,128)(2,1)S(1)}, bf16[512,2,2,2,32]{0,4,3,2,1:T(8,128)(2,1)}, u32[]{:S(2)}) copy-start(bf16[512,2,2,2,32]{0,4,3,2,1:T(8,128)(2,1)} %get-tuple-element.86) | copy-start | bytes 786436
  110.2 12.1 %copy-start.6 = (f32[2]{0:T(128)S(1)}, f32[2]{0:T(128)}, u32[]{:S(2)}) copy-start(f32[2]{0:T(128)} %param.23) | copy-start | bytes 28
  110.2 151.1 %reduce-scatter.2.cloned.1.call-start = ((), (), s32[]{:S(2)}) async-start(), calls=%async_computation.4 | async-start | bytes 4718592 | tf_op jit(solution)/shard_map/reduce_scatter | solution.py:146
  204.7 2.2 copy-start.2
  206.8 56.6 %copy-start.1 = (bf16[3,1024,512]{2,1,0:T(8,128)(2,1)S(1)}, bf16[3,1024,512]{2,1,0:T(8,128)(2,1)}, u32[]{:S(2)}) copy-start(bf16[3,1024,512]{2,1,0:T(8,128)(2,1)} %param.18) | copy-start | bytes 9437188
Sparse Core Ops, SparseCore 0:
  46.3 46.0 all-gather.5
  94.2 25.2 all-gather.3
  121.4 52.5 all-gather.7
  211.3 49.9 reduce-scatter.1
where the time goes:
time: 271 us; the launch traced here: 270 us
  waiting for transfers between devices  144 us (53%)
  matrix products  39.9 us (15%)
  blocking collectives  31.7 us (12%)
  other arithmetic  21.2 us (8%)
  local copies, waits for them, and re-layouts  19.3 us (7%)
  between operations  13.3 us (5%)
    reduce_scatter x1, waiting for transfers between devices, shards(): lax.psum_scatter(jnp.dot(attended, output_weight, preferred_element_type=...  50.1 us
    all_gather x1, waiting for transfers between devices, shards(): segment = lax.all_gather(packed, 'sp', axis=0, tiled=True)  46.9 us
    all_gather x1, waiting for transfers between devices, shards(): lax.all_gather(normed, 'tp', axis=0, tiled=True)  37.9 us
    psum x1, blocking collectives, shards(): summed = lax.psum(partial_mod, 'sp')  17.6 us
    all_gather x1, blocking collectives, shards(): mod_vectors = lax.all_gather(summed, 'tp', axis=2, tiled=True)  14.1 us
    dot_general x1, matrix products, shards(): jnp.dot(lax.all_gather(normed, 'tp', axis=0, tiled=True), projection, pre...  12.5 us
    dynamic_slice x4, local copies, waits for them, and re-layouts, shards(): lax.scan(one_block, state_now, stacked)[0]  11.9 us
    dot_general x3, matrix products, absorb(): jnp.einsum('mqhk,khd->mqhd', weights.astype(jnp.bfloat16), value_part, pr...  10.4 us
  transfers between devices with their start and end apart: 4, of which 4 were waited for; matrix products, arithmetic and copies ran while one was open for 12% of the time, Pallas kernels for 0%

commit v1 on v0

--- a/solution.py
+++ b/solution.py
@@ -84,7 +84,7 @@
     partial_mod = jnp.einsum(
         "cd,rde->cre", own_rows, modulation, preferred_element_type=jnp.float32
     )
-    summed = lax.psum(partial_mod, "sp")
+    summed = jnp.sum(lax.all_gather(partial_mod, "sp"), axis=0)
     mod_vectors = lax.all_gather(summed, "tp", axis=2, tiled=True)
     head_count = lambdas.shape[0]
     head_width = query_weight.shape[1] // head_count

time: 271 us -> 264 us (0.974)
  blocking collectives: 31.7 us -> 24 us
    psum x1 -> x0, blocking collectives: 17.6 us -> none  [shards(): summed = lax.psum(partial_mod, 'sp')]
    all_gather x0 -> x1, blocking collectives: none -> 9.85 us  [shards(): summed = jnp.sum(lax.all_gather(partial_mod, 'sp'), axis=0)]
  transfers between devices with their start and end apart: 4 -> 4, of which waited for: 4 -> 4; matrix products, arithmetic and copies ran while one was open for 12% -> 13% of each run, Pallas kernels for 0% -> 0%
where the time goes in v1:
time: 264 us; the launch traced here: 263 us
  waiting for transfers between devices  145 us (55%)
  matrix products  39.9 us (15%)
  blocking collectives  24 us (9%)
  other arithmetic  21.2 us (8%)
  local copies, waits for them, and re-layouts  19.3 us (7%)
  between operations  13.4 us (5%)
    reduce_scatter x1, waiting for transfers between devices, shards(): lax.psum_scatter(jnp.dot(attended, output_weight, preferred_element_type=...  50.1 us
    all_gather x1, waiting for transfers between devices, shards(): segment = lax.all_gather(packed, 'sp', axis=0, tiled=True)  46.9 us
    all_gather x1, waiting for transfers between devices, shards(): lax.all_gather(normed, 'tp', axis=0, tiled=True)  38.9 us
    all_gather x1, blocking collectives, shards(): mod_vectors = lax.all_gather(summed, 'tp', axis=2, tiled=True)  14.2 us
    dot_general x1, matrix products, shards(): jnp.dot(lax.all_gather(normed, 'tp', axis=0, tiled=True), projection, pre...  12.5 us
    dynamic_slice x4, local copies, waits for them, and re-layouts, shards(): lax.scan(one_block, state_now, stacked)[0]  11.9 us
    dot_general x3, matrix products, absorb(): jnp.einsum('mqhk,khd->mqhd', weights.astype(jnp.bfloat16), value_part, pr...  10.4 us
    all_gather x1, blocking collectives, shards(): summed = jnp.sum(lax.all_gather(partial_mod, 'sp'), axis=0)  9.85 us
  transfers between devices with their start and end apart: 4, of which 4 were waited for; matrix products, arithmetic and copies ran while one was open for 13% of the time, Pallas kernels for 0%

profile of v1, /device:TPU:0, one launch (start us, length us, event | category | flops | bytes accessed | tf_op | source)
XLA Modules:
  0.0 263.2 jit_solution(8848866607551969156)
XLA Ops:
  6.5 1.9 copy-done
  8.4 1.3 fusion.61
  9.7 9.8 %all-gather = f32[8,3,512]{2,1,0:T(4,128)S(1)} all-gather(f32[2,3,512]{2,1,0:T(4,128)S(1)} %copy.41), channel_id=2, replica_groups=mesh['sp'=4,'tp'=8] {'sp'}, dimensions={0}, use_global_device_ids=true | all-gather | bytes 61440 | tf_op jit(solution)/shard_map/all_gather | solution.py:87
  19.6 14.2 %all_gather.20 = f32[2,3,4096]{2,0,1:T(2,128)S(1)} all-gather(f32[2,3,512]{2,0,1:T(2,128)S(1)} %copy.67), channel_id=1, replica_groups=mesh['sp'=4,'tp'=8] {'tp'}, dimensions={2}, use_global_device_ids=true | all-gather | bytes 110592 | tf_op jit(solution)/shard_map/all_gather | solution.py:88
  35.1 1.3 fusion.40
  36.4 2.1 fusion.43
  38.6 1.5 convert_reduce_fusion
  40.5 5.0 %fusion.37 = bf16[128,1024]{1,0:T(8,128)(2,1)} fusion(bf16[4096,512]{1,0:T(8,128)(2,1)} %param.21, bf16[4096,512]{1,0:T(8,128)(2,1)} %param.20, bf16[128,4096]{1,0:T(8,128)(2,1)S(1)} %copy-done.3, f32[4096]{0:T(1024)S(1)} %bitcast.122, f32[4096]{0:T(1024)S(1)} %bitcast.123, f32[128]{0:T(128)S(1)} %add_rsqrt_fusion.2, f32[128]{0:T(128)S(1)} %broadcast_multiply_fusion.3), kind=kOutput, calls=%fused_computation.47 | convolution fusion | flops 1093795840 | bytes 9733120 | tf_op jit(solution)/shard_map/dot_general | solution.py:119
  46.8 38.9 %all-gather.7.cloned.1.call-done = bf16[512,4096]{1,0:T(8,128)(2,1)} async-done(((bf16[64,4096]{1,0:T(8,128)(2,1)}), bf16[512,4096]{1,0:T(8,128)(2,1)}) %all-gather.7.cloned.1.call-update) | async-done | bytes 4194320 | tf_op jit(solution)/shard_map/all_gather | solution.py:97
  85.7 12.5 %fusion.22 = bf16[512,1536]{1,0:T(8,128)(2,1)S(1)} fusion(bf16[512,4096]{1,0:T(8,128)(2,1)} %all-gather.7.cloned.1.call-done, bf16[4096,512]{1,0:T(8,128)(2,1)} %param.21, bf16[4096,512]{1,0:T(8,128)(2,1)} %param.20, bf16[4096,512]{1,0:T(8,128)(2,1)} %param.19), kind=kOutput, calls=%fused_computation.30 | convolution fusion | flops 6480986112 | bytes 18350080 | tf_op jit(solution)/shard_map/dot_general | solution.py:96
  100.0 2.0 subtract_convert_fusion
  103.8 9.1 %all-gather.5.cloned.1.call-done = bf16[512,1024]{1,0:T(8,128)(2,1)} async-done(((bf16[128,1024]{1,0:T(8,128)(2,1)}), bf16[512,1024]{1,0:T(8,128)(2,1)}) %all-gather.5.cloned.1.call-update) | async-done | bytes 1048592 | tf_op jit(solution)/shard_map/all_gather | solution.py:122
  112.8 1.3 fusion.77
  115.5 1.8 bitcast_reduce_fusion.1
  118.3 2.0 bitcast_add_fusion.1
  120.4 46.9 %all-gather.9.cloned.1.call-done = bf16[2048,1024]{1,0:T(8,128)(2,1)} async-done(((bf16[512,1024]{1,0:T(8,128)(2,1)}), bf16[2048,1024]{1,0:T(8,128)(2,1)}) %all-gather.9.cloned.1.call-update) | async-done | bytes 4194320 | tf_op jit(solution)/shard_map/all_gather | solution.py:129
  167.3 28.7 %while.14 = (s32[]{:T(128)}, f32[2,512,2]{1,2,0:T(2,128)S(1)}, f32[2,512,2]{1,2,0:T(2,128)S(1)}, f32[2,512,2,256]{1,3,0,2:T(8,128)}, bf16[2,1024,1024]{2,1,0:T(8...) while((s32[]{:T(128)}, f32[2,512,2]{1,2,0:T(2,128)S(1)}, f32[2,512,2]{1,2,0:T(2,128)S(1)}, ...), condition=%wide.region_10.11_spmd, body=%wide.region_7.10_spmd.sunk | while | flops 1624248320 | bytes 44703824 | solution.py:137
  167.3 3.1 %constant_dynamic-slice_fusion.2 = bf16[1,1024,1024]{2,1,0:T(8,128)(2,1)} fusion(bf16[2,1024,1024]{2,1,0:T(8,128)(2,1)} %get-tuple-element.179, s32[]{:T(128)} %get-tuple-element.168), kind=kLoop, calls=%fused_computation.12.clone.1 | loop fusion | bytes 4194308 | tf_op jit(solution)/shard_map/while/body/jit(dynamic_index_in_dim)/dynamic_slice | solution.py:137
  170.4 2.9 %copy.93 = bf16[1,1024,1024]{1,2,0:T(8,128)(2,1)S(1)} copy(bf16[1,1024,1024]{2,1,0:T(8,128)(2,1)} %constant_dynamic-slice_fusion.2) | data formatting | bytes 4194304 | tf_op jit(solution)/shard_map/while/body/jit(dynamic_index_in_dim)/dynamic_slice | solution.py:137
  173.4 2.4 bitcast_reduce_fusion.3
  175.8 1.6 fusion.96
  177.5 4.2 %bitcast_add_fusion.3 = f32[2,512,2,256]{1,3,0,2:T(8,128)} fusion(f32[2,512,2,256]{1,3,0,2:T(8,128)} %get-tuple-element.171, bf16[1024,2,256,1]{0,2,3,1:T(8,128)(2,1)S(1)} %bitcast.108, bf16[2,512,2,1024]{1,3,2,0:T(8,128)(2,1)S(1)} %get-tuple-element.159, f32[2,512,2]{1,0,2:T(2,128)S(1)} %copy.94), kind=kOutput, calls=%fused_computation.7.clone.1 | convolution fusion | flops 1074790400 | bytes 9445376 | tf_op jit(solution)/shard_map/while/body/eval_jaxpr/mqhk,khd->mqhd/dot_general | solution.py:57
  181.6 3.1 %constant_dynamic-slice_fusion.2 = bf16[1,1024,1024]{2,1,0:T(8,128)(2,1)} fusion(bf16[2,1024,1024]{2,1,0:T(8,128)(2,1)} %get-tuple-element.179, s32[]{:T(128)} %get-tuple-element.168), kind=kLoop, calls=%fused_computation.12.clone.1 | loop fusion | bytes 4194308 | tf_op jit(solution)/shard_map/while/body/jit(dynamic_index_in_dim)/dynamic_slice | solution.py:137
  184.7 2.9 %copy.93 = bf16[1,1024,1024]{1,2,0:T(8,128)(2,1)S(1)} copy(bf16[1,1024,1024]{2,1,0:T(8,128)(2,1)} %constant_dynamic-slice_fusion.2) | data formatting | bytes 4194304 | tf_op jit(solution)/shard_map/while/body/jit(dynamic_index_in_dim)/dynamic_slice | solution.py:137
  187.8 2.4 bitcast_reduce_fusion.3
  190.2 1.6 fusion.96
  191.8 4.2 %bitcast_add_fusion.3 = f32[2,512,2,256]{1,3,0,2:T(8,128)} fusion(f32[2,512,2,256]{1,3,0,2:T(8,128)} %get-tuple-element.171, bf16[1024,2,256,1]{0,2,3,1:T(8,128)(2,1)S(1)} %bitcast.108, bf16[2,512,2,1024]{1,3,2,0:T(8,128)(2,1)S(1)} %get-tuple-element.159, f32[2,512,2]{1,0,2:T(2,128)S(1)} %copy.94), kind=kOutput, calls=%fused_computation.7.clone.1 | convolution fusion | flops 1074790400 | bytes 9445376 | tf_op jit(solution)/shard_map/while/body/eval_jaxpr/mqhk,khd->mqhd/dot_general | solution.py:57
  196.0 1.9 broadcast_divide_fusion
  198.8 1.3 copy-done.2
  200.1 4.3 %convolution_convert_fusion = bf16[512,4096]{1,0:T(8,128)(2,1)} fusion(bf16[512,512]{0,1:T(8,128)(2,1)S(1)} %fusion.50, bf16[512,4096]{1,0:T(8,128)(2,1)S(1)} %copy-done.2), kind=kOutput, calls=%fused_computation.23 | convolution fusion | flops 2149580800 | bytes 8912896 | tf_op jit(solution)/shard_map/dot_general | solution.py:147
  204.4 50.1 %reduce-scatter.2.cloned.1.call-done = bf16[64,4096]{1,0:T(8,128)(2,1)} async-done(((bf16[512,4096]{1,0:T(8,128)(2,1)}), bf16[64,4096]{1,0:T(8,128)(2,1)}) %reduce-scatter.2.cloned.1.call-update) | async-done | bytes 524304 | tf_op jit(solution)/shard_map/reduce_scatter | solution.py:146
  254.5 2.1 fusion.44
  (70 shorter events, 10.3 us)
Async XLA Ops:
  6.5 1.9 copy-start
  6.5 79.1 %all-gather.7.cloned.1.call-start = ((), (), s32[]{:S(2)}) async-start(), calls=%async_computation.2 | async-start | bytes 4718592 | tf_op jit(solution)/shard_map/all_gather | solution.py:97
  9.7 30.4 %copy-start.3 = (bf16[128,4096]{1,0:T(8,128)(2,1)S(1)}, bf16[128,4096]{1,0:T(8,128)(2,1)}, u32[]{:S(2)}) copy-start(bf16[128,4096]{1,0:T(8,128)(2,1)} %param.15) | copy-start | bytes 3145732
  38.5 74.3 %all-gather.5.cloned.1.call-start = ((), (), s32[]{:S(2)}) async-start(), calls=%async_computation.1 | async-start | bytes 1310720 | tf_op jit(solution)/shard_map/all_gather | solution.py:122
  45.5 121.8 %all-gather.9.cloned.1.call-start = ((), (), s32[]{:S(2)}) async-start(), calls=%async_computation.3 | async-start | bytes 5242880 | tf_op jit(solution)/shard_map/all_gather | solution.py:129
  99.9 2.3 copy-start.4
  102.0 1.7 copy-start.7
  102.0 1.8 copy-start.8
  102.0 12.4 %copy-start.5 = (bf16[512,2,2,2,32]{0,4,3,2,1:T(8,128)(2,1)S(1)}, bf16[512,2,2,2,32]{0,4,3,2,1:T(8,128)(2,1)}, u32[]{:S(2)}) copy-start(bf16[512,2,2,2,32]{0,4,3,2,1:T(8,128)(2,1)} %get-tuple-element.92) | copy-start | bytes 786436
  103.4 12.1 %copy-start.6 = (f32[2]{0:T(128)S(1)}, f32[2]{0:T(128)}, u32[]{:S(2)}) copy-start(f32[2]{0:T(128)} %param.23) | copy-start | bytes 28
  103.4 151.1 %reduce-scatter.2.cloned.1.call-start = ((), (), s32[]{:S(2)}) async-start(), calls=%async_computation.4 | async-start | bytes 4718592 | tf_op jit(solution)/shard_map/reduce_scatter | solution.py:146
  197.9 2.2 copy-start.2
  200.1 56.6 %copy-start.1 = (bf16[3,1024,512]{2,1,0:T(8,128)(2,1)S(1)}, bf16[3,1024,512]{2,1,0:T(8,128)(2,1)}, u32[]{:S(2)}) copy-start(bf16[3,1024,512]{2,1,0:T(8,128)(2,1)} %param.18) | copy-start | bytes 9437188
Sparse Core Ops, SparseCore 0:
  38.7 46.9 all-gather.6
  87.5 25.2 all-gather.4
  114.7 52.5 all-gather.8
  204.6 49.9 reduce-scatter.1
